TPU v7x, 256 devices: a whole 4x4x8 slice. The times are simulated.
256 devices in a mesh: ep: 64 (over z, y, core), tp: 4 (over x).
Axes of the slice: x: 4, y: 4, z: 8, core: 2. Of those that a mesh axis runs over, the one named last changes fastest.
Arguments:
- tokens: bfloat16 [16384, 2048], P('ep'), may hold values from -6 to 6
- norm_gain: float32 [2048], replicated, may hold values from 0.1 to 1.9
- expert_ids: int32 [16384, 2], P('ep'), may hold values from 0 to 31, all different within a row; in each aligned block of 256 rows (0 to 255, 256 to 511, ...) at most 20 rows name the same one
- route_weight: float32 [16384, 2], P('ep'), may hold values from 0.2 to 1
- w_gate: bfloat16 [64, 2048, 3584], P('ep', None, 'tp'), may hold values from -0.125 to 0.125
- w_up: bfloat16 [64, 2048, 3584], P('ep', None, 'tp'), may hold values from -0.125 to 0.125
- w_down: bfloat16 [64, 3584, 2048], P('ep', 'tp'), may hold values from -0.0625 to 0.0625
Outputs:
- mixed: bfloat16 [16384, 2048], P('ep', 'tp')
Inputs may be any that keep to these rules, and one draw needn't show every extreme that they name: `expert_ids`: A token names 2 different experts. In each aligned block of 256 tokens (the tokens of one index of ep) no expert is named by more than 20 tokens, a bound that some block reaches.
All inputs are finite; a program needn't handle non-finite values.
Results may differ from a plain program's by a relative error of at most 0.014.
Values may be sent and summed in bfloat16 or wider, within the bound.
A program may use at most 128 MiB of HBM per device.

v0:
```python
import jax
import jax.numpy as jnp
from jax import lax
from jax.sharding import Mesh
from jax.sharding import PartitionSpec as P

HALVES = 2
EP = ("ep_0", "ep_1", "ep_2")


EPSILON = 1e-05


def split_up(array, dim, count):
    lengths = array.shape
    parts = array.reshape(*lengths[:dim], count, lengths[dim] // count, *lengths[dim + 1 :])
    return jnp.moveaxis(parts, dim, 0)


def in_order(parts, dim):
    parts = jnp.moveaxis(parts, 0, dim)
    lengths = parts.shape
    return parts.reshape(*lengths[:dim], lengths[dim] * lengths[dim + 1], *lengths[dim + 2 :])


def exchange_in_order(parts, axes, order):
    inside = parts.shape[1:]
    out = parts.reshape(*(lax.axis_size(a) for a in axes), *inside)
    for k in order:
        out = lax.all_to_all(out, axes[k], k, k, tiled=True)
    return out.reshape(-1, *inside)


def two_step_exchange(array, groups, order, split_dim, concat_dim):
    count = lax.axis_size(groups[0]) * lax.axis_size(groups[1])
    parts = split_up(array, split_dim, count)
    return in_order(exchange_in_order(parts, groups, order), concat_dim)


def swapped(value, axis, distance):
    mask = 2**distance
    pairs = [(source, source ^ mask) for source in range(lax.axis_size(axis))]
    return lax.ppermute(value, axis, pairs)


def sent_and_summed(array, axis, dim):
    count = lax.axis_size(axis)
    parts = lax.all_to_all(split_up(array, dim, count), axis, 0, 0, tiled=True)
    return jnp.sum(parts.astype(jnp.float32), axis=0)


def layer_normed(tokens, norm_gain):
    values = tokens.astype(jnp.float32)
    center = values - jnp.mean(values, axis=-1, keepdims=True)
    spread = jnp.mean(center * center, axis=-1, keepdims=True)
    return (center * lax.rsqrt(spread + EPSILON) * norm_gain).astype(jnp.bfloat16)


def slot_numbers(chosen, experts):
    onehot = (chosen[..., None] == jnp.arange(experts, dtype=jnp.int32)).astype(jnp.int32)
    before = jnp.cumsum(onehot, axis=1) - onehot
    return jnp.sum(before * onehot, axis=-1)


def body(tokens, norm_gain, expert_ids, route_weight, w_gate, w_up, w_down):
    tok_rows, width = tokens.shape
    top_count = expert_ids.shape[1]
    ep_count = lax.axis_size(EP)
    experts = ep_count // HALVES
    capacity = 2 * min(tok_rows // 2, 5 * tok_rows * top_count // (8 * experts))
    normed = layer_normed(tokens, norm_gain)
    padded = jnp.concatenate([normed, jnp.zeros((1, width), jnp.bfloat16)], axis=0)
    slots = slot_numbers(expert_ids.reshape(1, -1), experts).reshape(-1)
    flat_expert = expert_ids.reshape(-1)
    owner = jnp.arange(tok_rows * top_count, dtype=jnp.int32) // top_count
    place = flat_expert * capacity + slots
    table = jnp.full((experts * capacity,), tok_rows, jnp.int32).at[place].set(owner)
    outgoing = padded[table].reshape(experts, capacity, width)
    halved = outgoing.reshape(experts * HALVES, capacity // HALVES, width)
    mine = two_step_exchange(halved, (("ep_0", "ep_1"), "ep_2"), (0, 1), 0, 0)
    other = swapped(mine, EP, 0)
    is_first = lax.axis_index(EP) % 2 == 0
    leading = jnp.where(is_first, mine, other)
    trailing = jnp.where(is_first, other, mine)
    arrived = jnp.concatenate([leading, trailing], axis=1)
    routed = arrived.reshape(-1, width)
    gate = jnp.dot(routed, w_gate[0], preferred_element_type=jnp.float32)
    up = jnp.dot(routed, w_up[0], preferred_element_type=jnp.float32)
    hidden = (jax.nn.silu(gate) * up).astype(jnp.bfloat16)
    partial_value = jnp.dot(hidden, w_down[0], preferred_element_type=jnp.float32)
    reduced = sent_and_summed(partial_value.astype(jnp.bfloat16), "tp", 1).astype(jnp.bfloat16)
    returned = lax.all_to_all(
        reduced.reshape(ep_count, capacity, -1), EP, split_axis=0, concat_axis=0, tiled=True
    )
    quarter = returned.shape[2]
    summed = returned.reshape(experts, HALVES, capacity, quarter).astype(jnp.float32).sum(axis=1)
    picked = summed.reshape(experts * capacity, quarter)[place].reshape(
        tok_rows, top_count, quarter
    )
    mixed = jnp.sum(route_weight[:, :, None] * picked, axis=1)
    return mixed.astype(jnp.bfloat16)


def solution(mesh):
    finer = Mesh(mesh.devices.reshape(8, 4, 2, mesh.shape["tp"]), ("ep_0", "ep_1", "ep_2", "tp"))
    in_specs = (
        P(EP, None),
        P(),
        P(EP, None),
        P(EP, None),
        P(EP, None, "tp"),
        P(EP, None, "tp"),
        P(EP, "tp", None),
    )
    out_specs = P(EP, "tp")
    return jax.shard_map(body, mesh=finer, in_specs=in_specs, out_specs=out_specs, check_vma=False)
```

profile of v0, /device:TPU:32, one launch (start us, length us, event | category | flops | bytes accessed | tf_op | source)
XLA Modules:
  0.0 283.1 jit_solution(11001555768529312184)
XLA Ops:
  0.0 0.0 copy-start
  0.0 0.0 copy-start.1
  0.0 0.9 copy.27
  0.9 0.1 eq.33
  1.1 0.1 compare_convert_fusion
  1.1 1.2 reduce-window.6
  2.3 0.2 slice_reduce_fusion
  2.5 0.1 copy.29
  2.6 0.7 broadcast_multiply_fusion
  3.3 0.1 copy.30
  3.4 0.1 copy.26
  3.5 0.1 mul.69
  3.7 0.1 broadcast.114
  3.8 0.1 fusion.9
  3.9 2.4 scatter_custom_fusion
  6.4 1.4 convert_reduce_fusion.1
  7.9 1.6 fusion.6
  9.5 0.0 copy-done
  9.5 0.0 copy-done.1
  9.5 0.4 fusion.8
  9.9 0.1 concatenate.6
  10.0 4.1 %gather_fusion = bf16[640,2048]{1,0:T(8,128)(2,1)} fusion(bf16[257,2048]{1,0:T(8,128)(2,1)S(1)} %concatenate.6, s32[1024]{0:T(1024)S(1)} %pad_clamp_fusion.1), kind=kCustom, calls=%fused_computation | custom fusion | bytes 5245440 | tf_op jit(solution)/shard_map/gather | solution.py:78
  14.1 5.4 %reshape_reshape_reshape_reshape.3 = bf16[32,2,1,10,2048]{4,3,1,0,2:T(8,128)(2,1)} reshape(bf16[640,2048]{1,0:T(8,128)(2,1)} %gather_fusion) | data formatting | bytes 5242880 | tf_op jit(solution)/shard_map/reshape;reshape;reshape;reshape | solution.py:28
  19.5 4.9 %copy.31 = bf16[32,2,1,10,2048]{4,1,3,2,0:T(2,128)(2,1)S(1)} copy(bf16[32,2,1,10,2048]{4,3,1,0,2:T(8,128)(2,1)} %reshape_reshape_reshape_reshape.3) | data formatting | bytes 5242880 | tf_op jit(solution)/shard_map/reshape;reshape;reshape;reshape | solution.py:28
  24.4 73.4 %all_to_all.20 = bf16[32,2,1,10,2048]{4,1,3,2,0:T(2,128)(2,1)S(1)} all-to-all(bf16[32,2,1,10,2048]{4,1,3,2,0:T(2,128)(2,1)S(1)} %copy.31), channel_id=1, replica_groups=mesh['ep_0'=8,'ep_1'=4,'ep_2'=2,'tp'=4] {'ep_0','ep_1'}, dimensions={0} | all-to-all | bytes 5242880 | tf_op jit(solution)/shard_map/all_to_all | solution.py:30
  97.8 1.4 copy.32
  99.2 5.8 %all_to_all.21 = bf16[32,2,1,10,2048]{4,0,3,2,1:T(8,128)(2,1)S(1)} all-to-all(bf16[32,2,1,10,2048]{4,0,3,2,1:T(8,128)(2,1)S(1)} %copy.32), channel_id=1, replica_groups=mesh['ep_0'=8,'ep_1'=4,'ep_2'=2,'tp'=4] {'ep_2'}, dimensions={1} | all-to-all | bytes 5242880 | tf_op jit(solution)/shard_map/all_to_all | solution.py:30
  105.0 2.7 copy.33
  107.8 3.0 %reshape_reshape.3 = bf16[64,10,2048]{2,0,1:T(8,128)(2,1)} reshape(bf16[32,2,1,10,2048]{4,1,0,3,2:T(2,128)(2,1)S(1)} %copy.33) | data formatting | bytes 5242880 | tf_op jit(solution)/shard_map/reshape;reshape | solution.py:23
  110.8 0.2 collective-permute-start
  111.0 4.9 %collective-permute-done = bf16[64,10,2048]{2,0,1:T(8,128)(2,1)S(1)} collective-permute-done((bf16[64,10,2048]{2,0,1:T(8,128)(2,1)}, bf16[64,10,2048]{2,0,1:T(8,128)(2,1)S(1)}, u32[]{:S(2)}, u32[]{:S(2)}) %collective-permute-start) | collective-permute-done | bytes 2621472 | tf_op jit(solution)/shard_map/ppermute | solution.py:43
  115.9 2.1 broadcast_select_fusion.1
  118.0 0.5 pad_maximum_fusion
  118.4 5.6 %copy.34 = bf16[64,20,2048]{2,1,0:T(8,128)(2,1)} copy(bf16[64,20,2048]{2,0,1:T(8,128)(2,1)S(1)} %pad_maximum_fusion) | data formatting | bytes 10485760 | tf_op jit(solution)/shard_map/concatenate | solution.py:85
  124.1 9.0 %reshape.183 = bf16[1280,2048]{1,0:T(8,128)(2,1)} reshape(bf16[64,20,2048]{2,1,0:T(8,128)(2,1)} %copy.34) | data formatting | bytes 10485760 | tf_op jit(solution)/shard_map/reshape | solution.py:86
  133.1 10.0 %fusion.2 = f32[1280,896]{1,0:T(8,128)} fusion(bf16[1280,2048]{1,0:T(8,128)(2,1)} %reshape.183, bf16[1,2048,896]{2,1,0:T(8,128)(2,1)} %param.11), kind=kOutput, calls=%fused_computation.9 | convolution fusion | flops 4697620480 | bytes 13500416 | tf_op jit(solution)/shard_map/dot_general | solution.py:87
  143.0 17.6 %convolution_convert_fusion = bf16[1280,2048]{1,0:T(8,128)(2,1)} fusion(bf16[1,896,2048]{2,1,0:T(8,128)(2,1)} %param.13, f32[1280,896]{1,0:T(8,128)} %fusion.2, bf16[1280,2048]{1,0:T(8,128)(2,1)} %reshape.183, bf16[1,2048,896]{2,1,0:T(8,128)(2,1)} %param.12), kind=kOutput, calls=%fused_computation.3 | convolution fusion | flops 9404743680 | bytes 22413312 | tf_op jit(solution)/shard_map/dot_general | solution.py:90
  160.6 3.0 %copy.38 = bf16[160,4,8,512]{3,2,0,1:T(8,128)(2,1)S(1)} copy(bf16[160,4,8,512]{3,2,1,0:T(8,128)(2,1)} %bitcast.49) | data formatting | bytes 10485760 | tf_op jit(solution)/shard_map/reshape | solution.py:16
  163.6 64.6 %all_to_all.22 = bf16[4,1280,512]{2,1,0:T(8,128)(2,1)} all-to-all(bf16[4,1280,512]{2,1,0:T(8,128)(2,1)S(1)} %bitcast.48), channel_id=1, replica_groups=mesh['ep_0'=8,'ep_1'=4,'ep_2'=2,'tp'=4] {'tp'}, dimensions={0} | all-to-all | bytes 10485760 | tf_op jit(solution)/shard_map/all_to_all | solution.py:48
  228.2 4.2 %reduce_sum.63 = bf16[1280,512]{1,0:T(8,128)(2,1)S(1)} reduce(bf16[4,1280,512]{2,1,0:T(8,128)(2,1)} %all_to_all.22, bf16[]{:T(256)} %constant.65.clone.1), dimensions={0}, to_apply=%region_6.7 | reduce | flops 1966080 | bytes 6553602 | tf_op jit(solution)/shard_map/reduce_sum | solution.py:49
  232.4 0.0 copy-start.2
  232.4 1.3 reshape.185
  233.7 5.5 %all-to-all-start.3 = ((bf16[64,20,512]{2,1,0:T(8,128)(2,1)}), bf16[64,20,512]{2,1,0:T(8,128)(2,1)S(1)}, u32[]{:S(2)}, u32[]{:S(2)}) async-start(bf16[64,20,512]{2,1,0:T(8,128)(2,1)} %reshape.185), calls=%async_computation.3 | async-start | bytes 3145728 | tf_op jit(solution)/shard_map/all_to_all | solution.py:92
  239.2 0.0 copy-done.2
  239.2 0.1 copy.25
  239.4 39.0 %all-to-all-done.3 = bf16[64,20,512]{2,1,0:T(8,128)(2,1)S(1)} async-done(((bf16[64,20,512]{2,1,0:T(8,128)(2,1)}), bf16[64,20,512]{2,1,0:T(8,128)(2,1)S(1)}, u32[]{:S(2)}, u32[]{:S(2)}) %all-to-all-start.3) | async-done | bytes 1310752 | tf_op jit(solution)/shard_map/all_to_all | solution.py:92
  278.4 0.3 convert_reduce_fusion
  278.7 0.1 reshape.186
  278.8 1.6 gather_fusion.1
  280.4 0.6 reshape.187
  281.1 2.1 multiply_reduce_fusion
  (10 shorter events, 0.1 us)
Async XLA Ops:
  0.0 9.5 %copy-start = (bf16[256,2048]{1,0:T(8,128)(2,1)S(1)}, bf16[256,2048]{1,0:T(8,128)(2,1)}, u32[]{:S(2)}) copy-start(bf16[256,2048]{1,0:T(8,128)(2,1)} %param.7) | copy-start | bytes 3145732
  0.0 9.5 %copy-start.1 = (f32[2048]{0:T(1024)S(1)}, f32[2048]{0:T(1024)}, u32[]{:S(2)}) copy-start(f32[2048]{0:T(1024)} %param.8) | copy-start | bytes 24580
  110.8 5.1 %collective-permute-start = (bf16[64,10,2048]{2,0,1:T(8,128)(2,1)}, bf16[64,10,2048]{2,0,1:T(8,128)(2,1)S(1)}, u32[]{:S(2)}, u32[]{:S(2)}) collective-permute-start(bf16[64,10,2048]{2,0,1:T(8,128)(2,1)} %reshape_reshape.3), channel_id=1, source_target_pairs={{0,4},{4,0},{8,12},{12,8},{16,20},{20,16},{24,28},{28,24},{32,36},... | collective-permute-start | bytes 7864328 | tf_op jit(solution)/shard_map/ppermute | solution.py:43
  232.4 6.9 %copy-start.2 = (f32[256,2]{0,1:T(2,128)S(1)}, f32[256,2]{0,1:T(2,128)}, u32[]{:S(2)}) copy-start(f32[256,2]{0,1:T(2,128)} %param.10) | copy-start | bytes 6148
  233.7 44.7 %all-to-all-start.3 = ((bf16[64,20,512]{2,1,0:T(8,128)(2,1)}), bf16[64,20,512]{2,1,0:T(8,128)(2,1)S(1)}, u32[]{:S(2)}, u32[]{:S(2)}) async-start(bf16[64,20,512]{2,1,0:T(8,128)(2,1)} %reshape.185), calls=%async_computation.3 | async-start | bytes 3145728 | tf_op jit(solution)/shard_map/all_to_all | solution.py:92
where the time goes:
time: 285 us; the launch traced here: 283 us
  blocking collectives  144 us (51%)
  local copies, waits for them, and re-layouts  47.3 us (17%)
  waiting for transfers between devices  43.9 us (15%)
  matrix products  27.5 us (10%)
  other arithmetic  14.6 us (5%)
  starting transfers between devices  5.74 us (2%)
    all_to_all x2, blocking collectives, exchange_in_order(): out = lax.all_to_all(out, axes[k], k, k, tiled=True)  79.2 us
    all_to_all x1, blocking collectives, sent_and_summed(): parts = lax.all_to_all(split_up(array, dim, count), axis, 0, 0, tiled=True)  64.6 us
    all_to_all x1, waiting for transfers between devices, body(): lax.all_to_all(reduced.reshape(ep_count, capacity, -1), EP, split_axis=0,...  39 us
    dot_general x1, matrix products, body(): jnp.dot(hidden, w_down[0], preferred_element_type=jnp.float32)  17.6 us
    another operation x2, local copies, waits for them, and re-layouts, exchange_in_order(): out = parts.reshape(*(lax.axis_size(a) for a in axes), *inside)  10.3 us
    dot_general x1, matrix products, body(): gate = jnp.dot(routed, w_gate[0], preferred_element_type=jnp.float32)  9.98 us
    reshape x1, local copies, waits for them, and re-layouts, body(): routed = arrived.reshape(-1, width)  9 us
  transfers between devices with their start and end apart: 2, of which 2 were waited for; matrix products, arithmetic and copies ran while one was open for 0% of the time, Pallas kernels for 0%

commit v1 on v0

v1 whole, which is shorter than its diff:
```python
import jax
import jax.numpy as jnp
from jax import lax
from jax.experimental import pallas as pl
from jax.experimental.pallas import tpu as pltpu
from jax.sharding import PartitionSpec as P

MESH = pl.DeviceIdType.MESH
F32, BF16, I32 = jnp.float32, jnp.bfloat16, jnp.int32
EPSILON = 1e-05

NZ, NY, NX = 8, 4, 4
EXPERTS = NZ * NY
TOK = 256
D = 2048
CAP = 20
LANES = 128
DQ = D // NX
NJ = DQ // LANES
SLAB = CAP * NJ
BLOCK_H = 896
NT = BLOCK_H // LANES

GROUPS = ((1, 7), (0, 4), (2, 6), (3, 5))
NG = len(GROUPS)
PER = len(GROUPS[0])
HALF = PER * NY * CAP
ROWS = 2 * HALF
QUARTERS = (2, 1, 3, 0)


def place_numbers(ids):
    lanes = lax.broadcasted_iota(I32, (TOK, LANES), 1)
    named = [ids[:, k : k + 1] == lanes for k in range(2)]
    counts = (named[0].astype(F32) + named[1].astype(F32)).astype(BF16)
    rows = lax.broadcasted_iota(I32, (TOK, TOK), 0)
    cols = lax.broadcasted_iota(I32, (TOK, TOK), 1)
    earlier = jnp.where(cols < rows, 1.0, 0.0).astype(BF16)
    before = jnp.dot(earlier, counts, preferred_element_type=F32)
    slots = [jnp.sum(jnp.where(m, before, 0.0), axis=1, keepdims=True).astype(I32) for m in named]
    return [ids[:, k : k + 1] * CAP + slots[k] for k in range(2)]


def pre_kernel(tok_ref, gain_ref, ids_ref, out_ref, rows_ref, slab_ref):
    x = lax.axis_index("tp")
    columns = pl.ds(pl.multiple_of(x * DQ, DQ), DQ)
    values = tok_ref[...].astype(F32)
    mean = jnp.mean(values, axis=-1, keepdims=True)
    center = values - mean
    spread = jnp.mean(center * center, axis=-1, keepdims=True)
    quarter = tok_ref[:, columns].astype(F32) - mean
    normed = (quarter * lax.rsqrt(spread + EPSILON) * gain_ref[:, columns]).astype(BF16)
    place = place_numbers(ids_ref[...])
    cols = lax.broadcasted_iota(I32, (TOK, EXPERTS * CAP), 1)
    chosen = jnp.where((cols == place[0]) | (cols == place[1]), 1.0, 0.0).astype(BF16)
    rows_ref[...] = lax.dot_general(
        chosen, normed, (((0,), (0,)), ((), ())), preferred_element_type=F32
    )
    for e in range(EXPERTS):
        for j in range(NJ):
            slab_ref[pl.ds(e * SLAB + j * CAP, CAP), :] = rows_ref[
                pl.ds(e * CAP, CAP), pl.ds(j * LANES, LANES)
            ]
    out_ref[...] = slab_ref[...].reshape(EXPERTS, SLAB, LANES).astype(BF16)


def post_kernel(back_ref, ids_ref, weight_ref, out_ref, slab_ref, rows_ref):
    slab_ref[...] = back_ref[...].reshape(EXPERTS * SLAB, LANES).astype(F32)
    for e in range(EXPERTS):
        for j in range(NJ):
            rows_ref[pl.ds(e * CAP, CAP), pl.ds(j * LANES, LANES)] = slab_ref[
                pl.ds(e * SLAB + j * CAP, CAP), :
            ]
    rows = rows_ref[...].astype(BF16)
    place = place_numbers(ids_ref[...])
    cols = lax.broadcasted_iota(I32, (TOK, EXPERTS * CAP), 1)
    total = jnp.zeros((TOK, DQ), F32)
    for k in range(2):
        chosen = jnp.where(cols == place[k], 1.0, 0.0).astype(BF16)
        picked = jnp.dot(chosen, rows, preferred_element_type=F32)
        total = total + weight_ref[:, k : k + 1] * picked
    out_ref[...] = total.astype(BF16)


def main_kernel(
    out_slabs, wg_hbm, wu_hbm, wd_hbm, result,
    wgu, wd, arrived, routed, hidden, slabs, rows,
    own, psend, precv, t1, u1, t2, u2, ysend, back,
    w_sem, d_send, d_recv, ag_send, ag_recv, p_send, p_recv,
    r1_send, r1_recv, r2_send, r2_recv, y_send, y_recv,
):
    x = lax.axis_index("tp")
    ep = lax.axis_index("ep")
    core = lax.rem(ep, 2)
    expert = ep // 2
    y = lax.rem(expert, NY)
    z = expert // NY
    right, left = {"tp": lax.rem(x + 1, NX)}, {"tp": lax.rem(x + NX - 1, NX)}
    partner = {"ep": ep + 1 - 2 * core}

    def chip(to_z, to_y):
        return {"ep": (to_z * NY + to_y) * 2 + core}

    def remote(src, dst, send, recv, device):
        return pltpu.make_async_remote_copy(
            src_ref=src, dst_ref=dst, send_sem=send, recv_sem=recv,
            device_id=device, device_id_type=MESH,
        )

    def weight_copies():
        copies = []
        for n in range(NT):
            tile = pl.ds(n * LANES, LANES)
            for k, w in enumerate((wg_hbm, wu_hbm)):
                copies.append(
                    pltpu.make_async_copy(
                        w.at[0, :, tile], wgu.at[n, :, pl.ds(k * LANES, LANES)], w_sem.at[2 * n + k]
                    )
                )
        copies.append(pltpu.make_async_copy(wd_hbm.at[0], wd, w_sem.at[2 * NT]))
        return copies

    for copy in weight_copies():
        copy.start()

    barrier = pltpu.get_barrier_semaphore()

    def greet(i, carry):
        other = lax.rem(expert + i, EXPERTS)
        pl.semaphore_signal(
            barrier, inc=1, device_id={"ep": other * 2 + core}, device_id_type=MESH
        )
        return carry

    lax.fori_loop(1, EXPERTS, greet, 0)
    for device in (right, left, partner):
        pl.semaphore_signal(barrier, inc=1, device_id=device, device_id_type=MESH)
    pl.semaphore_wait(barrier, EXPERTS - 1 + 3)

    for g, offsets in enumerate(GROUPS):
        for d, dz in enumerate(offsets):
            to_z = lax.rem(z + dz, NZ)
            for dy in range(NY):
                to_y = lax.rem(y + dy, NY)
                if dz == 0 and dy == 0:
                    continue
                remote(
                    out_slabs.at[to_z * NY + to_y], arrived.at[g, d, y],
                    d_send, d_recv.at[g], chip(to_z, to_y),
                ).start()
            if dz == 0:
                arrived[g, d, y] = out_slabs[expert]

    def wait_slabs(sem, count, recv):
        span = pl.ds(0, count)
        copy = remote(out_slabs.at[span], back.at[span], sem, sem, partner)
        copy.wait_recv() if recv else copy.wait_send()

    def quarter_columns(q):
        return pl.ds(pl.multiple_of(q * DQ, DQ), DQ)

    q_own, q_left, q_right, q_far = (
        x, lax.rem(x + NX - 1, NX), lax.rem(x + 1, NX), lax.rem(x + 2, NX)
    )

    own_rows, other_rows = pl.ds(0, HALF), pl.ds(HALF, HALF)
    first, second = pl.ds(0, HALF // 2), pl.ds(HALF // 2, HALF // 2)

    def gather_copy(g, index):
        q, span, device = (
            (q_own, own_rows, right),
            (q_own, own_rows, left),
            (q_left, first, right),
            (q_right, second, left),
            (q_own, None, partner),
            (q_left, None, partner),
            (q_right, None, partner),
            (q_far, None, partner),
        )[index]
        columns = quarter_columns(q)
        src = routed.at[g, own_rows if span is None else span, columns]
        dst = routed.at[g, other_rows if span is None else span, columns]
        return remote(src, dst, ag_send.at[g, index], ag_recv.at[g, index], device)

    def gather_start(g):
        wait_slabs(d_recv.at[g], PER * NY - (1 if 0 in GROUPS[g] else 0), True)
        slabs[...] = arrived[g].reshape(PER * NY * SLAB, LANES).astype(F32)
        for i in range(PER * NY):
            for j in range(NJ):
                rows[pl.ds(i * CAP, CAP), pl.ds(j * LANES, LANES)] = slabs[
                    pl.ds(i * SLAB + j * CAP, CAP), :
                ]
        routed[g, own_rows, quarter_columns(q_own)] = rows[...].astype(BF16)
        for index in (0, 1, 4):
            gather_copy(g, index).start()

    def gather_forward(g):
        gather_copy(g, 0).wait_recv()
        gather_copy(g, 2).start()
        gather_copy(g, 5).start()
        gather_copy(g, 1).wait_recv()
        gather_copy(g, 3).start()
        gather_copy(g, 6).start()

    def gather_finish(g):
        gather_copy(g, 2).wait_recv()
        gather_copy(g, 3).wait_recv()
        gather_copy(g, 7).start()

    def gather_partner(g):
        for index in range(4, 8):
            gather_copy(g, index).wait_recv()

    def up_part(g):
        def step(n, carry):
            both = jnp.dot(routed[g], wgu[n], preferred_element_type=F32)
            gate, up = both[:, :LANES], both[:, LANES:]
            value = gate / (1.0 + jnp.exp(-gate)) * up
            hidden[:, pl.ds(pl.multiple_of(n * LANES, LANES), LANES)] = value.astype(BF16)
            return carry

        lax.fori_loop(0, NT, step, 0)

    def partial_copy(g, k):
        return remote(
            psend.at[g, k], precv.at[g, k], p_send.at[g, k], p_recv.at[g, k], partner
        )

    def down_part(g):
        for k, off in enumerate(QUARTERS):
            value = jnp.dot(
                hidden[...], wd[:, quarter_columns(lax.rem(x + off, NX))],
                preferred_element_type=F32,
            )
            psend[g, k] = value[HALF:].astype(BF16)
            own[g, k] = value[:HALF]
            partial_copy(g, k).start()

    def first_copy(g, way):
        span = (first, second)[way]
        return remote(
            t1.at[g, span], u1.at[g, span], r1_send.at[g, way], r1_recv.at[g, way], (right, left)[way]
        )

    def second_copy(g, way):
        return remote(
            t2.at[g, way], u2.at[g, way], r2_send.at[g, way], r2_recv.at[g, way], (right, left)[way]
        )

    def reduce_first(g):
        partial_copy(g, 0).wait_recv()
        t1[g] = (own[g, 0] + precv[g, 0].astype(F32)).astype(BF16)
        for way in range(2):
            first_copy(g, way).start()

    def reduce_second(g):
        for way, spans in enumerate(((first, second), (second, first))):
            partial_copy(g, 1 + way).wait_recv()
            first_copy(g, way).wait_recv()
            added, plain = spans
            t2[g, way, added] = (
                own[g, 1 + way, added] + precv[g, 1 + way, added].astype(F32)
                + u1[g, added].astype(F32)
            ).astype(BF16)
            t2[g, way, plain] = (
                own[g, 1 + way, plain] + precv[g, 1 + way, plain].astype(F32)
            ).astype(BF16)
            second_copy(g, way).start()

    def reduce_last(g):
        partial_copy(g, 3).wait_recv()
        second_copy(g, 0).wait_recv()
        second_copy(g, 1).wait_recv()
        rows[...] = (
            own[g, 3] + precv[g, 3].astype(F32) + u2[g, 0].astype(F32) + u2[g, 1].astype(F32)
        )
        for i in range(PER * NY):
            for j in range(NJ):
                slabs[pl.ds(i * SLAB + j * CAP, CAP), :] = rows[
                    pl.ds(i * CAP, CAP), pl.ds(j * LANES, LANES)
                ]
        ysend[g] = slabs[...].reshape(PER, NY, SLAB, LANES).astype(BF16)
        for d, dz in enumerate(GROUPS[g]):
            to_z = lax.rem(z + NZ - dz, NZ)
            for dy in range(NY):
                to_y = lax.rem(y + dy, NY)
                if dz == 0 and dy == 0:
                    back[expert] = ysend[g, d, y]
                    continue
                remote(
                    ysend.at[g, d, to_y], back.at[expert], y_send, y_recv, chip(to_z, to_y)
                ).start()

    gather_start(0)
    gather_start(1)
    gather_forward(0)
    gather_start(2)
    gather_finish(0)
    gather_forward(1)
    gather_start(3)
    for copy in weight_copies():
        copy.wait()
    gather_partner(0)
    up_part(0)
    gather_finish(1)
    gather_forward(2)
    down_part(0)
    gather_finish(2)
    gather_forward(3)
    gather_partner(1)
    up_part(1)
    reduce_first(0)
    gather_finish(3)
    down_part(1)
    reduce_second(0)
    gather_partner(2)
    up_part(2)
    reduce_first(1)
    reduce_last(0)
    down_part(2)
    reduce_second(1)
    gather_partner(3)
    up_part(3)
    reduce_first(2)
    reduce_last(1)
    down_part(3)
    reduce_second(2)
    reduce_first(3)
    reduce_last(2)
    reduce_second(3)
    reduce_last(3)

    wait_slabs(d_send, EXPERTS - 1, False)
    for g in range(NG):
        for index in range(8):
            gather_copy(g, index).wait_send()
        for k in range(4):
            partial_copy(g, k).wait_send()
        for way in range(2):
            first_copy(g, way).wait_send()
            second_copy(g, way).wait_send()
    wait_slabs(y_send, EXPERTS - 1, False)
    wait_slabs(y_recv, EXPERTS - 1, True)
    result[...] = back[...]


def body(tokens, norm_gain, expert_ids, route_weight, w_gate, w_up, w_down):
    vmem = pl.BlockSpec(memory_space=pltpu.VMEM)
    hbm = pl.BlockSpec(memory_space=pl.ANY)
    slab_array = jax.ShapeDtypeStruct((EXPERTS, SLAB, LANES), BF16)
    params = dict(vmem_limit_bytes=60 * 1024 * 1024)
    out_slabs = pl.pallas_call(
        pre_kernel,
        out_shape=slab_array,
        in_specs=[vmem] * 3,
        out_specs=vmem,
        scratch_shapes=[
            pltpu.VMEM((EXPERTS * CAP, DQ), F32),
            pltpu.VMEM((EXPERTS * SLAB, LANES), F32),
        ],
        compiler_params=pltpu.CompilerParams(**params),
    )(tokens, norm_gain.reshape(1, D), expert_ids)

    dma = pltpu.SemaphoreType.DMA
    returned = pl.pallas_call(
        main_kernel,
        out_shape=slab_array,
        in_specs=[vmem, hbm, hbm, hbm],
        out_specs=vmem,
        scratch_shapes=[
            pltpu.VMEM((NT, D, 2 * LANES), BF16),
            pltpu.VMEM((BLOCK_H, D), BF16),
            pltpu.VMEM((NG, PER, NY, SLAB, LANES), BF16),
            pltpu.VMEM((NG, ROWS, D), BF16),
            pltpu.VMEM((ROWS, BLOCK_H), BF16),
            pltpu.VMEM((PER * NY * SLAB, LANES), F32),
            pltpu.VMEM((HALF, DQ), F32),
            pltpu.VMEM((NG, 4, HALF, DQ), F32),
            pltpu.VMEM((NG, 4, HALF, DQ), BF16),
            pltpu.VMEM((NG, 4, HALF, DQ), BF16),
            pltpu.VMEM((NG, HALF, DQ), BF16),
            pltpu.VMEM((NG, HALF, DQ), BF16),
            pltpu.VMEM((NG, 2, HALF, DQ), BF16),
            pltpu.VMEM((NG, 2, HALF, DQ), BF16),
            pltpu.VMEM((NG, PER, NY, SLAB, LANES), BF16),
            pltpu.VMEM((EXPERTS, SLAB, LANES), BF16),
            dma((2 * NT + 1,)),
            dma,
            dma((NG,)),
            dma((NG, 8)),
            dma((NG, 8)),
            dma((NG, 4)),
            dma((NG, 4)),
            dma((NG, 2)),
            dma((NG, 2)),
            dma((NG, 2)),
            dma((NG, 2)),
            dma,
            dma,
        ],
        compiler_params=pltpu.CompilerParams(
            collective_id=0, has_side_effects=True, **params
        ),
    )(out_slabs, w_gate, w_up, w_down)

    return pl.pallas_call(
        post_kernel,
        out_shape=jax.ShapeDtypeStruct((TOK, DQ), BF16),
        in_specs=[vmem] * 3,
        out_specs=vmem,
        scratch_shapes=[
            pltpu.VMEM((EXPERTS * SLAB, LANES), F32),
            pltpu.VMEM((EXPERTS * CAP, DQ), F32),
        ],
        compiler_params=pltpu.CompilerParams(**params),
    )(returned, expert_ids, route_weight)


def solution(mesh):
    in_specs = (
        P("ep", None),
        P(),
        P("ep", None),
        P("ep", None),
        P("ep", None, "tp"),
        P("ep", None, "tp"),
        P("ep", "tp", None),
    )
    return jax.shard_map(
        body, mesh=mesh, in_specs=in_specs, out_specs=P("ep", "tp"), check_vma=False
    )
```

time: 285 us -> 94 us (0.33)
  blocking collectives: 144 us -> 0 us
  Pallas kernels: 0 us -> 91.5 us
  local copies, waits for them, and re-layouts: 47.3 us -> 2.28 us
  waiting for transfers between devices: 43.9 us -> 0 us
  matrix products: 27.5 us -> 0 us
  other arithmetic: 14.6 us -> 0 us
  starting transfers between devices: 5.74 us -> 0 us
    all_to_all x3 -> x0, blocking collectives: 144 us -> none  [the longest x2 79.2 us: exchange_in_order(): out = lax.all_to_all(out, axes[k], k, k, tiled=True)]
    pallas_call x0 -> x3, Pallas kernels: none -> 91.5 us  [the longest x1 85.1 us: body(): pl.pallas_call(main_kernel, out_shape=slab_array, in_specs=[vmem, hbm, hb...]
    all_to_all x1 -> x0, waiting for transfers between devices: 39 us -> none  [body(): lax.all_to_all(reduced.reshape(ep_count, capacity, -1), EP, split_axis=0,...]
    dot_general x2 -> x0, matrix products: 27.5 us -> none  [the longest x1 17.6 us: body(): jnp.dot(hidden, w_down[0], preferred_element_type=jnp.float32)]
    reshape x6 -> x0, local copies, waits for them, and re-layouts: 14 us -> none  [the longest x1 9 us: body(): routed = arrived.reshape(-1, width)]
    another operation x7 -> x0, local copies, waits for them, and re-layouts: 13.5 us -> none  [the longest x2 10.3 us: exchange_in_order(): out = parts.reshape(*(lax.axis_size(a) for a in axes), *inside)]
    reduce_sum x6 -> x0, other arithmetic: 9.73 us -> none  [the longest x1 4.16 us: sent_and_summed(): return jnp.sum(parts.astype(jnp.float32), axis=0)]
    concatenate x2 -> x0, local copies, waits for them, and re-layouts: 5.71 us -> none  [the longest x1 5.64 us: body(): arrived = jnp.concatenate([leading, trailing], axis=1)]
  transfers between devices with their start and end apart: 2 -> 0, of which waited for: 2 -> 0; matrix products, arithmetic and copies ran while one was open for 0% -> 0% of each run, Pallas kernels for 0% -> 0%
where the time goes in v1:
time: 94 us; the launch traced here: 93.8 us
  Pallas kernels  91.5 us (97%)
  local copies, waits for them, and re-layouts  2.28 us (2%)
    pallas_call x1, Pallas kernels, body(): pl.pallas_call(main_kernel, out_shape=slab_array, in_specs=[vmem, hbm, hb...  85.1 us
    pallas_call x1, Pallas kernels, body(): pl.pallas_call(pre_kernel, out_shape=slab_array, in_specs=[vmem] * 3, out...  3.37 us
    pallas_call x1, Pallas kernels, body(): pl.pallas_call(post_kernel, out_shape=jax.ShapeDtypeStruct((TOK, DQ), BF1...  3.02 us
    unnamed x4, local copies, waits for them, and re-layouts  2.28 us

profile of v1, /device:TPU:32, one launch (start us, length us, event | category | flops | bytes accessed | tf_op | source)
XLA Modules:
  0.0 93.8 jit_solution(8728912464350328761)
XLA Ops:
  0.0 1.5 %copy.8.ids_ref = s32[256,2]{1,0:T(8,128)} copy(s32[256,2]{0,1:T(2,128)} %param.9) | data formatting | bytes 4096 | tf_op args[2]
  1.5 3.4 %shard_map.73.out_slabs = bf16[32,80,128]{2,1,0:T(8,128)(2,1)} custom-call(bf16[256,2048]{1,0:T(8,128)(2,1)} %tok_ref.1, f32[1,2048]{1,0:T(1,128)} %bitcast.1, s32[256,2]{1,0:T(8,128)} %copy.8.ids_ref), custom_call_target="tpu_custom_call" | custom-call | tf_op jit(solution)/shard_map/pallas_call | solution.py:352
  4.8 0.0 copy-start
  4.9 85.1 %shard_map.74.back_ref = bf16[32,80,128]{2,1,0:T(8,128)(2,1)} custom-call(bf16[32,80,128]{2,1,0:T(8,128)(2,1)} %shard_map.73.out_slabs, bf16[1,2048,896]{2,1,0:T(8,128)(2,1)} %wg_hbm.1, bf16[1,2048,896]{2,1,0:T(8,128)(2,1)} %wu_hbm.1, bf16[1,896,2048]{2,1,0:T(8,128)(2,1)} %wd_hbm.1), custom_call_target="tpu_custom_call" | custom-call | tf_op jit(solution)/shard_map/pallas_call | solution.py:365
  90.0 0.0 copy-done
  90.0 0.8 copy.10.weight_ref
  90.8 3.0 %shard_map.75 = bf16[256,512]{1,0:T(8,128)(2,1)} custom-call(bf16[32,80,128]{2,1,0:T(8,128)(2,1)} %shard_map.74.back_ref, s32[256,2]{1,0:T(8,128)} %copy.8.ids_ref, f32[256,2]{1,0:T(8,128)} %copy.10.weight_ref), custom_call_target="tpu_custom_call" | custom-call | tf_op jit(solution)/shard_map/pallas_call | solution.py:406
Async XLA Ops:
  4.8 85.1 %copy-start = (f32[256,2]{0,1:T(2,128)S(1)}, f32[256,2]{0,1:T(2,128)}, u32[]{:S(2)}) copy-start(f32[256,2]{0,1:T(2,128)} %param.10) | copy-start | bytes 6148

commit v2 on v0

v2 whole, which is shorter than its diff:
```python
import jax
import jax.numpy as jnp
from jax import lax
from jax.experimental import pallas as pl
from jax.experimental.pallas import tpu as pltpu
from jax.sharding import PartitionSpec as P

MESH = pl.DeviceIdType.MESH
F32, BF16, I32 = jnp.float32, jnp.bfloat16, jnp.int32
EPSILON = 1e-05

NZ, NY, NX = 8, 4, 4
EXPERTS = NZ * NY
TOK = 256
D = 2048
CAP = 20
LANES = 128
DQ = D // NX
NJ = DQ // LANES
SLAB = CAP * NJ
BLOCK_H = 896
NT = BLOCK_H // LANES
BLK = NY * CAP

GROUPS = ((2,), (5,), (7,), (4,), (3,), (6,), (1,), (0,))
ISSUE = (0, 3, 1, 4, 7, 5, 2, 6)
WHOLE = (2, 6, 7)
COMBINE = (0, 1, 2, 3, 4, 5, 6, 7)
ORDER = (
    ("start", 0),
    ("start", 1),
    ("forward", 0),
    ("start", 7),
    ("forward", 1),
    ("start", 5),
    ("finish", 0),
    ("weights",),
    ("ready", 0),
    ("up", 0, 0),
    ("start", 3),
    ("up", 0, 1),
    ("up", 0, 2),
    ("finish", 1),
    ("up", 0, 3),
    ("down", 0, 0),
    ("down", 0, 1),
    ("down", 0, 2),
    ("down", 0, 3),
    ("forward", 5),
    ("first", 0),
    ("ready", 1),
    ("up", 1, 0),
    ("start", 2),
    ("up", 1, 1),
    ("forward", 3),
    ("up", 1, 2),
    ("start", 4),
    ("up", 1, 3),
    ("down", 1, 0),
    ("down", 1, 1),
    ("down", 1, 2),
    ("down", 1, 3),
    ("finish", 5),
    ("first", 1),
    ("ready", 2),
    ("up", 2, 0),
    ("second", 0),
    ("up", 2, 1),
    ("up", 2, 2),
    ("finish", 3),
    ("up", 2, 3),
    ("down", 2, 0),
    ("down", 2, 1),
    ("down", 2, 2),
    ("forward", 4),
    ("down", 2, 3),
    ("first", 2),
    ("ready", 3),
    ("up", 3, 0),
    ("second", 1),
    ("start", 6),
    ("up", 3, 1),
    ("up", 3, 2),
    ("last", 0),
    ("up", 3, 3),
    ("down", 3, 0),
    ("down", 3, 1),
    ("finish", 4),
    ("down", 3, 2),
    ("down", 3, 3),
    ("first", 3),
    ("second", 2),
    ("ready", 4),
    ("up", 4, 0),
    ("up", 4, 1),
    ("up", 4, 2),
    ("last", 1),
    ("up", 4, 3),
    ("down", 4, 0),
    ("down", 4, 1),
    ("down", 4, 2),
    ("second", 3),
    ("down", 4, 3),
    ("first", 4),
    ("ready", 5),
    ("up", 5, 0),
    ("up", 5, 1),
    ("last", 2),
    ("up", 5, 2),
    ("up", 5, 3),
    ("down", 5, 0),
    ("down", 5, 1),
    ("down", 5, 2),
    ("down", 5, 3),
    ("ready", 6),
    ("up", 6, 0),
    ("first", 5),
    ("last", 3),
    ("up", 6, 1),
    ("second", 4),
    ("up", 6, 2),
    ("up", 6, 3),
    ("down", 6, 0),
    ("down", 6, 1),
    ("down", 6, 2),
    ("down", 6, 3),
    ("ready", 7),
    ("up", 7, 0),
    ("second", 5),
    ("first", 6),
    ("up", 7, 1),
    ("up", 7, 2),
    ("up", 7, 3),
    ("last", 4),
    ("down", 7, 0),
    ("down", 7, 1),
    ("down", 7, 2),
    ("down", 7, 3),
    ("first", 7),
    ("last", 5),
    ("second", 6),
    ("second", 7),
    ("last", 6),
    ("mix", 0),
    ("mix", 1),
    ("mix", 2),
    ("mix", 3),
    ("mix", 4),
    ("last", 7),
    ("mix", 5),
    ("mix", 6),
    ("mix", 7),
)
NG = len(GROUPS)
OFFSETS = tuple(dz for offsets in GROUPS for dz in offsets)
BASE = tuple(sum(len(o) for o in GROUPS[:g]) for g in range(NG))
SIZE = tuple(len(o) for o in GROUPS)
NF = len(WHOLE)
GATHERED = tuple(g for g in range(NG) if g not in WHOLE)
TOP_ROWS = 2 * BLK * max(SIZE)
CUTS = (0, 2, 4, 6, 7)
QUARTERS = (2, 1, 3, 0)
ALL_ROWS = EXPERTS * CAP
VMEM_BYTES = 53 * 1024 * 1024 + 256 * 1024


def main_kernel(
    tok_hbm, gain_ref, ids_ref, weight_ref, wg_hbm, wu_hbm, wd_hbm, result,
    tok, normed, full_slabs, full_in, out_slabs, arrived, mix_hi, mix_lo,
    wgu, wd, routed, acc, hidden, rows, slabs,
    own, psend, precv, t1, u1, t2, u2, ysend, back, total,
    tok_sem, w_sem, f_send, d_send, d_recv, ag_send, ag_recv, p_send, p_recv,
    r1_send, r1_recv, r2_send, r2_recv, y_send, y_recv,
):
    x = lax.axis_index("tp")
    ep = lax.axis_index("ep")
    core = lax.rem(ep, 2)
    expert = ep // 2
    y = lax.rem(expert, NY)
    z = expert // NY
    right, left = {"tp": lax.rem(x + 1, NX)}, {"tp": lax.rem(x + NX - 1, NX)}
    partner = {"ep": ep + 1 - 2 * core}

    def chip(to_z, to_y):
        return {"ep": (to_z * NY + to_y) * 2 + core}

    def remote(src, dst, send, recv, device):
        return pltpu.make_async_remote_copy(
            src_ref=src, dst_ref=dst, send_sem=send, recv_sem=recv,
            device_id=device, device_id_type=MESH,
        )

    def weight_copies():
        copies = []
        for n in range(NT):
            tile = pl.ds(n * LANES, LANES)
            for k, w in enumerate((wg_hbm, wu_hbm)):
                copies.append(
                    pltpu.make_async_copy(
                        w.at[0, :, tile], wgu.at[n, :, pl.ds(k * LANES, LANES)], w_sem.at[0]
                    )
                )
        copies.append(pltpu.make_async_copy(wd_hbm.at[0], wd, w_sem.at[1]))
        return copies

    tok_copy = pltpu.make_async_copy(tok_hbm, tok, tok_sem)
    tok_copy.start()

    barrier = pltpu.get_barrier_semaphore()

    def greet(i, carry):
        other = lax.rem(expert + i, EXPERTS)
        pl.semaphore_signal(
            barrier, inc=1, device_id={"ep": other * 2 + core}, device_id_type=MESH
        )
        return carry

    lax.fori_loop(1, EXPERTS, greet, 0)
    for device in (right, left, partner):
        pl.semaphore_signal(barrier, inc=1, device_id=device, device_id_type=MESH)
    for copy in weight_copies():
        copy.start()

    def rows_wait(sem, count, recv):
        copy = remote(t1.at[pl.ds(0, count)], u1.at[pl.ds(0, count)], sem, sem, partner)
        copy.wait_recv() if recv else copy.wait_send()

    def quarter_columns(q):
        return pl.ds(pl.multiple_of(q * DQ, DQ), DQ)

    ids = [ids_ref[k : k + 1, :] for k in range(2)]
    experts = lax.broadcasted_iota(I32, (EXPERTS, TOK), 0)
    named = [experts == ids[k] for k in range(2)]
    counts = (named[0].astype(F32) + named[1].astype(F32)).astype(BF16)
    token_from = lax.broadcasted_iota(I32, (TOK, TOK), 0)
    token_to = lax.broadcasted_iota(I32, (TOK, TOK), 1)
    earlier = jnp.where(token_from < token_to, 1.0, 0.0).astype(BF16)
    before = jnp.dot(counts, earlier, preferred_element_type=F32)
    place = []
    for k in range(2):
        slot = jnp.sum(jnp.where(named[k], before, 0.0), axis=0, keepdims=True).astype(I32)
        away = ((ids[k] >> 2) + (NZ - z)) & (NZ - 1)
        position = jnp.zeros_like(away)
        for at, dz in enumerate(OFFSETS):
            position = jnp.where(away == dz, at, position)
        place.append((position * NY + (ids[k] & (NY - 1))) * CAP + slot)
    row_index = lax.broadcasted_iota(I32, (ALL_ROWS, TOK), 0)
    hits = [row_index == place[k] for k in range(2)]
    chosen = jnp.where(hits[0] | hits[1], 1.0, 0.0).astype(BF16)

    tok_copy.wait()
    values = tok[...].astype(F32)
    center = values - jnp.mean(values, axis=-1, keepdims=True)
    spread = jnp.mean(center * center, axis=-1, keepdims=True)
    normed[...] = (center * lax.rsqrt(spread + EPSILON) * gain_ref[...]).astype(BF16)

    rows[...] = jnp.dot(chosen, normed[:, quarter_columns(x)], preferred_element_type=F32)
    for i in range(EXPERTS):
        if i // NY in [BASE[g] for g in WHOLE]:
            continue
        for j in range(NJ):
            slabs[pl.ds(i * SLAB + j * CAP, CAP), :] = rows[
                pl.ds(i * CAP, CAP), pl.ds(j * LANES, LANES)
            ]
    for g in range(NG):
        if g not in WHOLE:
            span = pl.ds(BASE[g] * NY, SIZE[g] * NY)
            out_slabs[span] = (
                slabs[pl.ds(BASE[g] * NY * SLAB, SIZE[g] * NY * SLAB)]
                .reshape(SIZE[g] * NY, SLAB, LANES)
                .astype(BF16)
            )
    for f, g in enumerate(WHOLE):
        near = chosen[BASE[g] * BLK : (BASE[g] + 1) * BLK]
        for q in range(NX):
            rows[0:BLK] = jnp.dot(
                near, normed[:, q * DQ : (q + 1) * DQ], preferred_element_type=F32
            )
            for i in range(NY):
                for j in range(NJ):
                    slabs[pl.ds(i * SLAB + j * CAP, CAP), :] = rows[
                        pl.ds(i * CAP, CAP), pl.ds(j * LANES, LANES)
                    ]
            full_slabs[f * NY : (f + 1) * NY, q] = (
                slabs[0 : NY * SLAB].reshape(NY, SLAB, LANES).astype(BF16)
            )

    pl.semaphore_wait(barrier, EXPERTS - 1 + 3)

    for g in ISSUE:
        if g in WHOLE:
            at = WHOLE.index(g) * NY
            for dy in range(NY):
                to_y = lax.rem(y + dy, NY)
                if dy or GROUPS[g][0]:
                    remote(
                        full_slabs.at[at + to_y], full_in.at[at + y], f_send, d_recv.at[g],
                        chip(lax.rem(z + GROUPS[g][0], NZ), to_y),
                    ).start()
                else:
                    full_in[at + y] = full_slabs[at + y]
            continue
        for d, dz in enumerate(GROUPS[g]):
            for dy in range(NY):
                to_y = lax.rem(y + dy, NY)
                at = (BASE[g] + d) * NY
                if dy or dz:
                    remote(
                        out_slabs.at[at + to_y], arrived.at[at + y],
                        d_send, d_recv.at[g], chip(lax.rem(z + dz, NZ), to_y),
                    ).start()
                else:
                    arrived[at + y] = out_slabs[at + y]
    mix = jnp.where(hits[0], weight_ref[0:1, :], 0.0) + jnp.where(hits[1], weight_ref[1:2, :], 0.0)
    high = mix.astype(BF16)
    mix_hi[...] = high
    mix_lo[...] = (mix - high.astype(F32)).astype(BF16)

    def wait_slabs(sem, count, recv):
        span = pl.ds(0, count)
        copy = remote(out_slabs.at[span], back.at[span], sem, sem, partner)
        copy.wait_recv() if recv else copy.wait_send()

    q_own, q_left, q_right, q_far = (
        x, lax.rem(x + NX - 1, NX), lax.rem(x + 1, NX), lax.rem(x + 2, NX)
    )

    def parts_of(g):
        count = SIZE[g] * BLK
        cut = -(-count // 32) * 16
        return (0, cut), (cut, count - cut)

    def shared(g, part):
        return pl.ds(BASE[g] * BLK + part[0], part[1])

    def gather_rows(g, part, other):
        start = BASE[g] * 2 * BLK + (SIZE[g] * BLK if other else 0)
        return pl.ds(start + part[0], part[1])

    def gather_copy(g, index):
        whole = (0, SIZE[g] * BLK)
        first, second = parts_of(g)
        q, part, device = (
            (q_own, whole, right),
            (q_own, whole, left),
            (q_left, first, right),
            (q_right, second, left),
            (q_own, whole, partner),
            (q_left, whole, partner),
            (q_right, whole, partner),
            (q_far, whole, partner),
        )[index]
        columns = pl.ds(0, D) if g in WHOLE else quarter_columns(q)
        src = routed.at[gather_rows(g, part, False), columns]
        dst = routed.at[gather_rows(g, part, index >= 4), columns]
        sent = 8 if g in WHOLE else index
        return remote(src, dst, ag_send.at[sent], ag_recv.at[g, (0, 1, 2, 2, 3, 3, 3, 3)[index]], device)

    def gather_start(g):
        if g in WHOLE:
            at = WHOLE.index(g) * NY
            wait_slabs(d_recv.at[g], (NY - (0 in GROUPS[g])) * NX, True)
            for q in range(NX):
                slabs[0 : NY * SLAB] = (
                    full_in[at : at + NY, q].reshape(NY * SLAB, LANES).astype(F32)
                )
                for i in range(NY):
                    for j in range(NJ):
                        rows[pl.ds(i * CAP, CAP), pl.ds(j * LANES, LANES)] = slabs[
                            pl.ds(i * SLAB + j * CAP, CAP), :
                        ]
                routed[gather_rows(g, (0, BLK), False), q * DQ : (q + 1) * DQ] = rows[
                    0:BLK
                ].astype(BF16)
            gather_copy(g, 4).start()
            return
        count = SIZE[g] * NY
        wait_slabs(d_recv.at[g], count - (0 in GROUPS[g]), True)
        span = pl.ds(BASE[g] * NY, count)
        slabs[0 : count * SLAB] = arrived[span].reshape(count * SLAB, LANES).astype(F32)
        for i in range(count):
            for j in range(NJ):
                rows[pl.ds(i * CAP, CAP), pl.ds(j * LANES, LANES)] = slabs[
                    pl.ds(i * SLAB + j * CAP, CAP), :
                ]
        routed[gather_rows(g, (0, count * CAP), False), quarter_columns(q_own)] = rows[
            0 : count * CAP
        ].astype(BF16)
        for index in (0, 1, 4):
            gather_copy(g, index).start()

    def gather_forward(g):
        gather_copy(g, 0).wait_recv()
        gather_copy(g, 2).start()
        gather_copy(g, 5).start()
        gather_copy(g, 1).wait_recv()
        gather_copy(g, 3).start()
        gather_copy(g, 6).start()

    def gather_finish(g):
        rows_wait(ag_recv.at[g, 2], SIZE[g] * BLK, True)
        gather_copy(g, 7).start()

    def gather_partner(g):
        span = gather_rows(g, (0, SIZE[g] * BLK), True)
        remote(
            routed.at[span], routed.at[span], ag_send.at[8], ag_recv.at[g, 3], partner
        ).wait_recv()

    def up_part(g, part):
        count = 2 * SIZE[g] * BLK
        span = pl.ds(BASE[g] * 2 * BLK, count)

        def activate(n):
            gate, up = acc[n % 2, 0:count, 0:LANES], acc[n % 2, 0:count, LANES:]
            value = gate / (1.0 + jnp.exp(-gate)) * up
            hidden[0:count, n * LANES : (n + 1) * LANES] = value.astype(BF16)

        for n in range(CUTS[part], CUTS[part + 1]):
            if n:
                activate(n - 1)
            acc[n % 2, 0:count] = jnp.dot(routed[span], wgu[n], preferred_element_type=F32)
        if CUTS[part + 1] == NT:
            activate(NT - 1)

    def partial_copy(g, k):
        span = shared(g, (0, SIZE[g] * BLK))
        return remote(
            psend.at[k, span], precv.at[k, span], p_send, p_recv.at[g, k], partner
        )

    def down_part(g, k):
        count = SIZE[g] * BLK
        span = shared(g, (0, count))
        value = jnp.dot(
            hidden[0 : 2 * count], wd[:, quarter_columns(lax.rem(x + QUARTERS[k], NX))],
            preferred_element_type=F32,
        )
        psend[k, span] = value[count:].astype(BF16)
        own[k, span] = value[:count]
        partial_copy(g, k).start()

    def first_copy(g, way):
        span = shared(g, parts_of(g)[way])
        return remote(
            t1.at[span], u1.at[span], r1_send, r1_recv.at[g, way], (right, left)[way]
        )

    def second_copy(g, way):
        span = shared(g, (0, SIZE[g] * BLK))
        return remote(
            t2.at[way, span], u2.at[way, span], r2_send, r2_recv.at[g],
            (right, left)[way],
        )

    def chip_sum(k, span):
        return own[k, span] + precv[k, span].astype(F32)

    def reduce_first(g):
        partial_copy(g, 0).wait_recv()
        span = shared(g, (0, SIZE[g] * BLK))
        t1[span] = chip_sum(0, span).astype(BF16)
        for way in range(2):
            first_copy(g, way).start()

    def reduce_second(g):
        for way in range(2):
            added, plain = (shared(g, parts_of(g)[p]) for p in (way, 1 - way))
            partial_copy(g, 1 + way).wait_recv()
            t2[way, plain] = chip_sum(1 + way, plain).astype(BF16)
            first_copy(g, way).wait_recv()
            t2[way, added] = (chip_sum(1 + way, added) + u1[added].astype(F32)).astype(BF16)
            second_copy(g, way).start()

    def reduce_last(g):
        count = SIZE[g] * BLK
        span = shared(g, (0, count))
        partial_copy(g, 3).wait_recv()
        remote(
            t2.at[:, span], u2.at[:, span], r2_send, r2_recv.at[g], partner
        ).wait_recv()
        rows[0:count] = chip_sum(3, span) + u2[0, span].astype(F32) + u2[1, span].astype(F32)
        for i in range(SIZE[g] * NY):
            for j in range(NJ):
                slabs[pl.ds(i * SLAB + j * CAP, CAP), :] = rows[
                    pl.ds(i * CAP, CAP), pl.ds(j * LANES, LANES)
                ]
        ysend[pl.ds(BASE[g] * NY, SIZE[g] * NY)] = (
            slabs[0 : SIZE[g] * NY * SLAB].reshape(SIZE[g] * NY, SLAB, LANES).astype(BF16)
        )
        for d, dz in enumerate(GROUPS[g]):
            at = (BASE[g] + d) * NY
            for dy in range(NY):
                to_y = lax.rem(y + dy, NY)
                if dz == 0 and dy == 0:
                    back[at + y] = ysend[at + y]
                    continue
                remote(
                    ysend.at[at + to_y], back.at[at + y], y_send, y_recv.at[g],
                    chip(lax.rem(z + NZ - dz, NZ), to_y),
                ).start()

    def combine(g):
        count = SIZE[g] * NY
        wait_slabs(y_recv.at[g], count - (0 in GROUPS[g]), True)
        slabs[0 : count * SLAB] = (
            back[pl.ds(BASE[g] * NY, count)].reshape(count * SLAB, LANES).astype(F32)
        )
        for i in range(count):
            for j in range(NJ):
                rows[pl.ds(i * CAP, CAP), pl.ds(j * LANES, LANES)] = slabs[
                    pl.ds(i * SLAB + j * CAP, CAP), :
                ]
        picked = rows[0 : count * CAP].astype(BF16)
        span = pl.ds(BASE[g] * BLK, count * CAP)
        value = sum(
            lax.dot_general(
                mix[span], picked, (((0,), (0,)), ((), ())), preferred_element_type=F32
            )
            for mix in (mix_hi, mix_lo)
        )
        if g == COMBINE[0]:
            total[...] = value
        elif g != COMBINE[-1]:
            total[...] += value
        else:
            result[...] = (total[...] + value).astype(BF16)

    def weights_wait():
        pltpu.make_async_copy(wgu, wgu, w_sem.at[0]).wait()
        pltpu.make_async_copy(wd, wd, w_sem.at[1]).wait()

    steps = {
        "start": gather_start,
        "forward": gather_forward,
        "finish": gather_finish,
        "weights": weights_wait,
        "ready": gather_partner,
        "up": up_part,
        "down": down_part,
        "first": reduce_first,
        "second": reduce_second,
        "last": reduce_last,
        "mix": combine,
    }
    for name, *which in ORDER:
        steps[name](*which)

    if NF:
        span = pl.ds(0, NF * NY - (0 in [GROUPS[g][0] for g in WHOLE]))
        remote(full_slabs.at[span], full_in.at[span], f_send, f_send, partner).wait_send()
        span = pl.ds(0, NF * BLK)
        remote(
            routed.at[span], routed.at[span], ag_send.at[8], ag_send.at[8], partner
        ).wait_send()
    gathered = sum(SIZE[g] for g in GATHERED)
    own_sent = 0 in [dz for g in GATHERED for dz in GROUPS[g]]
    wait_slabs(d_send, gathered * NY - own_sent, False)
    for index in range(8):
        count = gathered * BLK
        if index in (2, 3):
            count = sum(parts_of(g)[index - 2][1] for g in GATHERED)
        rows_wait(ag_send.at[index], count, False)
    remote(psend, precv, p_send, p_send, partner).wait_send()
    remote(t1, u1, r1_send, r1_send, partner).wait_send()
    remote(t2, u2, r2_send, r2_send, partner).wait_send()
    wait_slabs(y_send, EXPERTS - 1, False)


def body(tokens, norm_gain, expert_ids, route_weight, w_gate, w_up, w_down):
    vmem = pl.BlockSpec(memory_space=pltpu.VMEM)
    hbm = pl.BlockSpec(memory_space=pl.ANY)
    dma = pltpu.SemaphoreType.DMA
    return pl.pallas_call(
        main_kernel,
        out_shape=jax.ShapeDtypeStruct((TOK, DQ), BF16),
        in_specs=[hbm, vmem, vmem, vmem, hbm, hbm, hbm],
        out_specs=vmem,
        scratch_shapes=[
            pltpu.VMEM((TOK, D), BF16),
            pltpu.VMEM((TOK, D), BF16),
            pltpu.VMEM((max(NF, 1) * NY, NX, SLAB, LANES), BF16),
            pltpu.VMEM((max(NF, 1) * NY, NX, SLAB, LANES), BF16),
            pltpu.VMEM((EXPERTS, SLAB, LANES), BF16),
            pltpu.VMEM((EXPERTS, SLAB, LANES), BF16),
            pltpu.VMEM((ALL_ROWS, TOK), BF16),
            pltpu.VMEM((ALL_ROWS, TOK), BF16),
            pltpu.VMEM((NT, D, 2 * LANES), BF16),
            pltpu.VMEM((BLOCK_H, D), BF16),
            pltpu.VMEM((2 * ALL_ROWS, D), BF16),
            pltpu.VMEM((2, TOP_ROWS, 2 * LANES), F32),
            pltpu.VMEM((TOP_ROWS, BLOCK_H), BF16),
            pltpu.VMEM((ALL_ROWS, DQ), F32),
            pltpu.VMEM((EXPERTS * SLAB, LANES), F32),
            pltpu.VMEM((4, ALL_ROWS, DQ), F32),
            pltpu.VMEM((4, ALL_ROWS, DQ), BF16),
            pltpu.VMEM((4, ALL_ROWS, DQ), BF16),
            pltpu.VMEM((ALL_ROWS, DQ), BF16),
            pltpu.VMEM((ALL_ROWS, DQ), BF16),
            pltpu.VMEM((2, ALL_ROWS, DQ), BF16),
            pltpu.VMEM((2, ALL_ROWS, DQ), BF16),
            pltpu.VMEM((EXPERTS, SLAB, LANES), BF16),
            pltpu.VMEM((EXPERTS, SLAB, LANES), BF16),
            pltpu.VMEM((TOK, DQ), F32),
            dma,
            dma((2,)),
            dma,
            dma,
            dma((NG,)),
            dma((9,)),
            dma((NG, 4)),
            dma,
            dma((NG, 4)),
            dma,
            dma((NG, 2)),
            dma,
            dma((NG,)),
            dma,
            dma((NG,)),
        ],
        compiler_params=pltpu.CompilerParams(
            collective_id=0, has_side_effects=True, vmem_limit_bytes=VMEM_BYTES
        ),
    )(tokens, norm_gain.reshape(1, D), expert_ids.T, route_weight.T, w_gate, w_up, w_down)


def solution(mesh):
    in_specs = (
        P("ep", None),
        P(),
        P("ep", None),
        P("ep", None),
        P("ep", None, "tp"),
        P("ep", None, "tp"),
        P("ep", "tp", None),
    )
    return jax.shard_map(
        body, mesh=mesh, in_specs=in_specs, out_specs=P("ep", "tp"), check_vma=False
    )
```

time: 285 us -> 77.2 us (0.27)
  blocking collectives: 144 us -> 0 us
  Pallas kernels: 0 us -> 73.3 us
  local copies, waits for them, and re-layouts: 47.3 us -> 2.76 us
  waiting for transfers between devices: 43.9 us -> 0 us
  matrix products: 27.5 us -> 0 us
  other arithmetic: 14.6 us -> 0 us
  starting transfers between devices: 5.74 us -> 0 us
    all_to_all x3 -> x0, blocking collectives: 144 us -> none  [the longest x2 79.2 us: exchange_in_order(): out = lax.all_to_all(out, axes[k], k, k, tiled=True)]
    pallas_call x0 -> x1, Pallas kernels: none -> 73.3 us  [body(): pl.pallas_call(main_kernel, out_shape=jax.ShapeDtypeStruct((TOK, DQ), BF1...]
    all_to_all x1 -> x0, waiting for transfers between devices: 39 us -> none  [body(): lax.all_to_all(reduced.reshape(ep_count, capacity, -1), EP, split_axis=0,...]
    dot_general x2 -> x0, matrix products: 27.5 us -> none  [the longest x1 17.6 us: body(): jnp.dot(hidden, w_down[0], preferred_element_type=jnp.float32)]
    reshape x6 -> x0, local copies, waits for them, and re-layouts: 14 us -> none  [the longest x1 9 us: body(): routed = arrived.reshape(-1, width)]
    another operation x7 -> x0, local copies, waits for them, and re-layouts: 13.5 us -> none  [the longest x2 10.3 us: exchange_in_order(): out = parts.reshape(*(lax.axis_size(a) for a in axes), *inside)]
    reduce_sum x6 -> x0, other arithmetic: 9.73 us -> none  [the longest x1 4.16 us: sent_and_summed(): return jnp.sum(parts.astype(jnp.float32), axis=0)]
    concatenate x2 -> x0, local copies, waits for them, and re-layouts: 5.71 us -> none  [the longest x1 5.64 us: body(): arrived = jnp.concatenate([leading, trailing], axis=1)]
  transfers between devices with their start and end apart: 2 -> 0, of which waited for: 2 -> 0; matrix products, arithmetic and copies ran while one was open for 0% -> 0% of each run, Pallas kernels for 0% -> 0%
where the time goes in v2:
time: 77.2 us; the launch traced here: 76.1 us
  Pallas kernels  73.3 us (95%)
  local copies, waits for them, and re-layouts  2.76 us (4%)
    pallas_call x1, Pallas kernels, body(): pl.pallas_call(main_kernel, out_shape=jax.ShapeDtypeStruct((TOK, DQ), BF1...  73.3 us
    unnamed x7, local copies, waits for them, and re-layouts  2.76 us

profile of v2, /device:TPU:32, one launch (start us, length us, event | category | flops | bytes accessed | tf_op | source)
XLA Modules:
  0.0 76.1 jit_solution(3380457987784827970)
XLA Ops:
  0.0 0.0 copy-start
  0.0 0.7 copy-done
  0.7 0.0 copy-start.1
  0.7 0.7 copy-done.1
  1.4 0.0 copy-start.2
  1.4 0.7 copy-done.2
  2.1 73.3 %shard_map.73 = bf16[256,512]{1,0:T(8,128)(2,1)S(1)} custom-call(bf16[256,2048]{1,0:T(8,128)(2,1)} %tok_hbm.1, f32[1,2048]{1,0:T(1,128)S(1)} %bitcast.3, s32[2,256]{1,0:T(2,128)S(1)} %bitcast.4, f32[2,256]{1,0:T(2,128)S(1)} %bitcast.5, bf16[1,2048,896]{2,1,0:T(8,128)(2,1)} %wg_hbm.1, bf16[1,2048,896]{2,1,0:T(8,128)(2,1)} %wu_hbm.1, bf16[1,896,2048]{2,1,0:T(8,128)(2,1)} %wd_hbm.1), custom_call_target="tpu_custom_call" | custom-call | tf_op jit(solution)/shard_map/pallas_call | solution.py:574
  75.4 0.7 copy.9
Async XLA Ops:
  0.0 0.7 copy-start
  0.7 0.7 copy-start.1
  1.4 0.7 copy-start.2

commit v3 on v2

--- a/solution.py
+++ b/solution.py
@@ -22,134 +22,106 @@
 NT = BLOCK_H // LANES
 BLK = NY * CAP
 
-GROUPS = ((2,), (5,), (7,), (4,), (3,), (6,), (1,), (0,))
-ISSUE = (0, 3, 1, 4, 7, 5, 2, 6)
-WHOLE = (2, 6, 7)
-COMBINE = (0, 1, 2, 3, 4, 5, 6, 7)
+GROUPS = ((0,), (2, 6), (4,), (5, 3), (1,), (7,))
+ISSUE = (1, 0, 2, 3, 5, 4)
+WHOLE = (0, 4, 5)
+EARLY = 3
+COMBINE = (0, 1, 2, 3, 4, 5)
 ORDER = (
+    ("start", 1),
+    ("send", 3),
     ("start", 0),
-    ("start", 1),
-    ("forward", 0),
-    ("start", 7),
-    ("forward", 1),
-    ("start", 5),
-    ("finish", 0),
     ("weights",),
     ("ready", 0),
     ("up", 0, 0),
-    ("start", 3),
+    ("send", 5),
     ("up", 0, 1),
     ("up", 0, 2),
-    ("finish", 1),
+    ("send", 4),
+    ("start", 2),
     ("up", 0, 3),
     ("down", 0, 0),
     ("down", 0, 1),
     ("down", 0, 2),
     ("down", 0, 3),
-    ("forward", 5),
+    ("forward", 1),
     ("first", 0),
+    ("forward", 2),
+    ("start", 3),
+    ("finish", 1),
+    ("second", 0),
     ("ready", 1),
     ("up", 1, 0),
-    ("start", 2),
+    ("finish", 2),
     ("up", 1, 1),
-    ("forward", 3),
     ("up", 1, 2),
-    ("start", 4),
     ("up", 1, 3),
     ("down", 1, 0),
+    ("forward", 3),
     ("down", 1, 1),
     ("down", 1, 2),
     ("down", 1, 3),
-    ("finish", 5),
     ("first", 1),
+    ("last", 0),
     ("ready", 2),
     ("up", 2, 0),
-    ("second", 0),
     ("up", 2, 1),
     ("up", 2, 2),
-    ("finish", 3),
     ("up", 2, 3),
     ("down", 2, 0),
     ("down", 2, 1),
+    ("finish", 3),
     ("down", 2, 2),
-    ("forward", 4),
     ("down", 2, 3),
+    ("start", 5),
+    ("start", 4),
     ("first", 2),
     ("ready", 3),
     ("up", 3, 0),
     ("second", 1),
-    ("start", 6),
     ("up", 3, 1),
     ("up", 3, 2),
-    ("last", 0),
     ("up", 3, 3),
+    ("second", 2),
     ("down", 3, 0),
     ("down", 3, 1),
-    ("finish", 4),
     ("down", 3, 2),
     ("down", 3, 3),
     ("first", 3),
-    ("second", 2),
     ("ready", 4),
     ("up", 4, 0),
     ("up", 4, 1),
+    ("last", 1),
     ("up", 4, 2),
-    ("last", 1),
     ("up", 4, 3),
     ("down", 4, 0),
+    ("last", 2),
     ("down", 4, 1),
     ("down", 4, 2),
-    ("second", 3),
     ("down", 4, 3),
     ("first", 4),
     ("ready", 5),
     ("up", 5, 0),
+    ("second", 3),
     ("up", 5, 1),
-    ("last", 2),
     ("up", 5, 2),
     ("up", 5, 3),
     ("down", 5, 0),
     ("down", 5, 1),
     ("down", 5, 2),
     ("down", 5, 3),
-    ("ready", 6),
-    ("up", 6, 0),
     ("first", 5),
+    ("second", 4),
     ("last", 3),
-    ("up", 6, 1),
-    ("second", 4),
-    ("up", 6, 2),
-    ("up", 6, 3),
-    ("down", 6, 0),
-    ("down", 6, 1),
-    ("down", 6, 2),
-    ("down", 6, 3),
-    ("ready", 7),
-    ("up", 7, 0),
     ("second", 5),
-    ("first", 6),
-    ("up", 7, 1),
-    ("up", 7, 2),
-    ("up", 7, 3),
     ("last", 4),
-    ("down", 7, 0),
-    ("down", 7, 1),
-    ("down", 7, 2),
-    ("down", 7, 3),
-    ("first", 7),
-    ("last", 5),
-    ("second", 6),
-    ("second", 7),
-    ("last", 6),
     ("mix", 0),
     ("mix", 1),
     ("mix", 2),
+    ("last", 5),
     ("mix", 3),
     ("mix", 4),
-    ("last", 7),
     ("mix", 5),
-    ("mix", 6),
-    ("mix", 7),
 )
 NG = len(GROUPS)
 OFFSETS = tuple(dz for offsets in GROUPS for dz in offsets)
@@ -161,13 +133,13 @@
 CUTS = (0, 2, 4, 6, 7)
 QUARTERS = (2, 1, 3, 0)
 ALL_ROWS = EXPERTS * CAP
-VMEM_BYTES = 53 * 1024 * 1024 + 256 * 1024
+VMEM_BYTES = 53 * 1024 * 1024 + 512 * 1024
 
 
 def main_kernel(
     tok_hbm, gain_ref, ids_ref, weight_ref, wg_hbm, wu_hbm, wd_hbm, result,
     tok, normed, full_slabs, full_in, out_slabs, arrived, mix_hi, mix_lo,
-    wgu, wd, routed, acc, hidden, rows, slabs,
+    wgu, wd, routed, acc, hidden, rows, whole_rows, slabs,
     own, psend, precv, t1, u1, t2, u2, ysend, back, total,
     tok_sem, w_sem, f_send, d_send, d_recv, ag_send, ag_recv, p_send, p_recv,
     r1_send, r1_recv, r2_send, r2_recv, y_send, y_recv,
@@ -227,6 +199,13 @@
 
     def quarter_columns(q):
         return pl.ds(pl.multiple_of(q * DQ, DQ), DQ)
+
+    def to_slabs(src, src_row, dst, dst_row, count):
+        for i in range(count):
+            for j in range(NJ):
+                dst[pl.ds(dst_row + i * SLAB + j * CAP, CAP), :] = src[
+                    pl.ds(src_row + i * CAP, CAP), pl.ds(j * LANES, LANES)
+                ]
 
     ids = [ids_ref[k : k + 1, :] for k in range(2)]
     experts = lax.broadcasted_iota(I32, (EXPERTS, TOK), 0)
@@ -255,62 +234,54 @@
     normed[...] = (center * lax.rsqrt(spread + EPSILON) * gain_ref[...]).astype(BF16)
 
     rows[...] = jnp.dot(chosen, normed[:, quarter_columns(x)], preferred_element_type=F32)
-    for i in range(EXPERTS):
-        if i // NY in [BASE[g] for g in WHOLE]:
-            continue
-        for j in range(NJ):
-            slabs[pl.ds(i * SLAB + j * CAP, CAP), :] = rows[
-                pl.ds(i * CAP, CAP), pl.ds(j * LANES, LANES)
-            ]
-    for g in range(NG):
-        if g not in WHOLE:
-            span = pl.ds(BASE[g] * NY, SIZE[g] * NY)
-            out_slabs[span] = (
-                slabs[pl.ds(BASE[g] * NY * SLAB, SIZE[g] * NY * SLAB)]
-                .reshape(SIZE[g] * NY, SLAB, LANES)
-                .astype(BF16)
-            )
-    for f, g in enumerate(WHOLE):
-        near = chosen[BASE[g] * BLK : (BASE[g] + 1) * BLK]
-        for q in range(NX):
-            rows[0:BLK] = jnp.dot(
-                near, normed[:, q * DQ : (q + 1) * DQ], preferred_element_type=F32
-            )
-            for i in range(NY):
-                for j in range(NJ):
-                    slabs[pl.ds(i * SLAB + j * CAP, CAP), :] = rows[
-                        pl.ds(i * CAP, CAP), pl.ds(j * LANES, LANES)
-                    ]
-            full_slabs[f * NY : (f + 1) * NY, q] = (
-                slabs[0 : NY * SLAB].reshape(NY, SLAB, LANES).astype(BF16)
-            )
-
     pl.semaphore_wait(barrier, EXPERTS - 1 + 3)
 
-    for g in ISSUE:
+    def prepare(g):
         if g in WHOLE:
             at = WHOLE.index(g) * NY
-            for dy in range(NY):
-                to_y = lax.rem(y + dy, NY)
-                if dy or GROUPS[g][0]:
-                    remote(
-                        full_slabs.at[at + to_y], full_in.at[at + y], f_send, d_recv.at[g],
-                        chip(lax.rem(z + GROUPS[g][0], NZ), to_y),
-                    ).start()
-                else:
-                    full_in[at + y] = full_slabs[at + y]
-            continue
+            near = chosen[BASE[g] * BLK : (BASE[g] + 1) * BLK]
+            for q in range(NX):
+                part = pl.ds(q * BLK, BLK)
+                whole_rows[part] = jnp.dot(
+                    near, normed[:, q * DQ : (q + 1) * DQ], preferred_element_type=F32
+                )
+                to_slabs(whole_rows, q * BLK, slabs, q * NY * SLAB, NY)
+                full_slabs[at : at + NY, q] = (
+                    slabs[q * NY * SLAB : (q + 1) * NY * SLAB]
+                    .reshape(NY, SLAB, LANES)
+                    .astype(BF16)
+                )
+            return
+        first_slab, count = BASE[g] * NY, SIZE[g] * NY
+        to_slabs(rows, first_slab * CAP, slabs, first_slab * SLAB, count)
+        out_slabs[pl.ds(first_slab, count)] = (
+            slabs[pl.ds(first_slab * SLAB, count * SLAB)].reshape(count, SLAB, LANES).astype(BF16)
+        )
+
+    def dispatch(g):
         for d, dz in enumerate(GROUPS[g]):
             for dy in range(NY):
                 to_y = lax.rem(y + dy, NY)
-                at = (BASE[g] + d) * NY
+                if g in WHOLE:
+                    at = WHOLE.index(g) * NY
+                    src, dst, sent = full_slabs, full_in, f_send
+                else:
+                    at = (BASE[g] + d) * NY
+                    src, dst, sent = out_slabs, arrived, d_send
                 if dy or dz:
                     remote(
-                        out_slabs.at[at + to_y], arrived.at[at + y],
-                        d_send, d_recv.at[g], chip(lax.rem(z + dz, NZ), to_y),
+                        src.at[at + to_y], dst.at[at + y], sent, d_recv.at[g],
+                        chip(lax.rem(z + dz, NZ), to_y),
                     ).start()
                 else:
-                    arrived[at + y] = out_slabs[at + y]
+                    dst[at + y] = src[at + y]
+
+    for g in ISSUE[:EARLY]:
+        prepare(g)
+        dispatch(g)
+    for g in ISSUE[EARLY:]:
+        prepare(g)
+
     mix = jnp.where(hits[0], weight_ref[0:1, :], 0.0) + jnp.where(hits[1], weight_ref[1:2, :], 0.0)
     high = mix.astype(BF16)
     mix_hi[...] = high
@@ -531,6 +502,7 @@
         pltpu.make_async_copy(wd, wd, w_sem.at[1]).wait()
 
     steps = {
+        "send": dispatch,
         "start": gather_start,
         "forward": gather_forward,
         "finish": gather_finish,
@@ -591,6 +563,7 @@
             pltpu.VMEM((2, TOP_ROWS, 2 * LANES), F32),
             pltpu.VMEM((TOP_ROWS, BLOCK_H), BF16),
             pltpu.VMEM((ALL_ROWS, DQ), F32),
+            pltpu.VMEM((NX * BLK, DQ), F32),
             pltpu.VMEM((EXPERTS * SLAB, LANES), F32),
             pltpu.VMEM((4, ALL_ROWS, DQ), F32),
             pltpu.VMEM((4, ALL_ROWS, DQ), BF16),

time: 77.2 us -> 72.6 us (0.940)
  Pallas kernels: 73.3 us -> 69.1 us
    pallas_call x1, Pallas kernels: 73.3 us -> 69.1 us  [body(): pl.pallas_call(main_kernel, out_shape=jax.ShapeDtypeStruct((TOK, DQ), BF1...]
where the time goes in v3:
time: 72.6 us; the launch traced here: 71.9 us
  Pallas kernels  69.1 us (95%)
  local copies, waits for them, and re-layouts  2.76 us (4%)
    pallas_call x1, Pallas kernels, body(): pl.pallas_call(main_kernel, out_shape=jax.ShapeDtypeStruct((TOK, DQ), BF1...  69.1 us
    unnamed x7, local copies, waits for them, and re-layouts  2.76 us

profile of v3, /device:TPU:32, one launch (start us, length us, event | category | flops | bytes accessed | tf_op | source)
XLA Modules:
  0.0 71.9 jit_solution(13891336398617770469)
XLA Ops:
  0.0 0.0 copy-start
  0.0 0.7 copy-done
  0.7 0.0 copy-start.1
  0.7 0.7 copy-done.1
  1.4 0.0 copy-start.2
  1.4 0.7 copy-done.2
  2.1 69.1 %shard_map.73 = bf16[256,512]{1,0:T(8,128)(2,1)S(1)} custom-call(bf16[256,2048]{1,0:T(8,128)(2,1)} %tok_hbm.1, f32[1,2048]{1,0:T(1,128)S(1)} %bitcast.3, s32[2,256]{1,0:T(2,128)S(1)} %bitcast.4, f32[2,256]{1,0:T(2,128)S(1)} %bitcast.5, bf16[1,2048,896]{2,1,0:T(8,128)(2,1)} %wg_hbm.1, bf16[1,2048,896]{2,1,0:T(8,128)(2,1)} %wu_hbm.1, bf16[1,896,2048]{2,1,0:T(8,128)(2,1)} %wd_hbm.1), custom_call_target="tpu_custom_call" | custom-call | tf_op jit(solution)/shard_map/pallas_call | solution.py:546
  71.1 0.7 copy.9
Async XLA Ops:
  0.0 0.7 copy-start
  0.7 0.7 copy-start.1
  1.4 0.7 copy-start.2
